TPU v7x, 32 devices: a whole 2x2x4 slice. The times are simulated.
32 devices in a mesh: sp: 16 (over z, y, core), tp: 2 (over x).
Axes of the slice: x: 2, y: 2, z: 4, core: 2. Of those that a mesh axis runs over, the one named last changes fastest.
Arguments:
- tokens: bfloat16 [1024, 4, 2048], P(('sp', 'tp')), may hold values from -16 to 16
- norm_gain: float32 [2048], replicated, may hold values from 0.1 to 1.9
- w_query: bfloat16 [2048, 2048], P('sp', 'tp'), may hold values from -0.125 to 0.125
- w_forget: bfloat16 [2048, 2048], P('sp', 'tp'), may hold values from -0.125 to 0.125
- w_value: bfloat16 [2048, 2048], P('sp', 'tp'), may hold values from -0.125 to 0.125
- floor_gap: float32 [2048], P('tp'), may hold values from 0 to 0.15, as said below
- head_gain: float32 [2048], P('tp'), may hold values from 0.1 to 1.9
- w_out: bfloat16 [2048, 2048], P('tp', 'sp'), may hold values from -0.125 to 0.125
Outputs:
- mixed: bfloat16 [1024, 4, 2048], P(('sp', 'tp'))
Inputs may be any that keep to these rules, and one draw needn't show every extreme that they name: `floor_gap`: positive, at least 0.5 / 1024 and at most 0.15.
All inputs are finite; a program needn't handle non-finite values.
Results may differ from a plain program's by a relative error of at most 0.014.
Values may be sent and summed in bfloat16 or wider, within the bound.
A program may use at most 128 MiB of HBM per device.

v0:
```python
import math

import jax
import jax.numpy as jnp
from jax import lax
from jax.sharding import PartitionSpec as P

KEY_DIM = 128
VAL_DIM = 128


eps_norm = 1e-06
highest = lax.Precision.HIGHEST


def carried_in(value, axis, combine, identity):
    length, mine = (lax.axis_size(axis), lax.axis_index(axis))
    everything = jax.tree.map(lambda part: lax.all_gather(part, axis), value)
    start = jax.tree.map(
        lambda part, zero: jnp.broadcast_to(jnp.asarray(zero, part.dtype), part.shape),
        value,
        identity,
    )

    def hop(k, before):
        reached = k < mine
        new = combine(before, jax.tree.map(lambda part: part[k], everything))
        return jax.tree.map(lambda a, b: jnp.where(reached, a, b), new, before)

    return lax.fori_loop(0, length, hop, start)


def link_states(earlier, later):
    decay_early, state_early = earlier
    decay_late, state_late = later
    return (decay_early * decay_late, decay_late[..., None] * state_early + state_late)


def local_pass(query, inkey, log_forget, values):
    block_len = query.shape[1]
    cumulative = jnp.cumsum(log_forget, axis=1)
    final = cumulative[:, -1]
    query_scaled = query * jnp.exp(cumulative)
    key_scaled = inkey * jnp.exp(-cumulative)
    key_final = inkey * jnp.exp(final[:, None] - cumulative)
    scores = jnp.einsum("ntshk,nushk->nshtu", query_scaled, key_scaled, precision=highest)
    positions = lax.iota(jnp.int32, block_len)
    causal = positions[:, None] >= positions[None, :]
    scores = jnp.where(causal, scores, 0.0)
    inside = jnp.einsum("nshtu,nushv->ntshv", scores, values, precision=highest)
    updates = jnp.einsum("nushk,nushv->nshkv", key_final, values, precision=highest)
    block_decay = jnp.exp(final)

    def advance(carry, inputs):
        decay_block, update_block = inputs
        return (decay_block[..., None] * carry + update_block, carry)

    end_state, entering = lax.scan(advance, jnp.zeros_like(updates[0]), (block_decay, updates))
    inside = inside + jnp.einsum("ntshk,nshkv->ntshv", query_scaled, entering, precision=highest)
    offsets = jnp.cumsum(final, axis=0) - final
    reach = query_scaled * jnp.exp(offsets)[:, None]
    total_decay = jnp.exp(jnp.sum(final, axis=0))
    return (inside, reach, total_decay, end_state)


def read_out(reach, incoming):
    return jnp.einsum("ntshk,shkv->ntshv", reach, incoming, precision=highest)


def body(tokens, norm_gain, w_query, w_forget, w_value, floor_gap, head_gain, w_out):
    flat = tokens.astype(jnp.float32)
    scale = lax.rsqrt(jnp.mean(flat * flat, axis=-1, keepdims=True) + eps_norm)
    normed = (flat * scale * norm_gain).astype(jnp.bfloat16)
    whole_query, whole_forget, whole_value = (
        lax.all_gather(w_query, "sp", axis=0, tiled=True),
        lax.all_gather(w_forget, "sp", axis=0, tiled=True),
        lax.all_gather(w_value, "sp", axis=0, tiled=True),
    )
    key_width = whole_query.shape[1]
    piece = lax.all_gather(normed, "tp", axis=0, tiled=True)
    flat_rows = piece.reshape(-1, piece.shape[-1])
    outputs = [
        jnp.dot(flat_rows, weight, preferred_element_type=jnp.float32).astype(jnp.bfloat16)
        for weight in (whole_query, whole_forget, whole_value)
    ]
    joined = jnp.concatenate(outputs, axis=1)
    projected = joined.reshape(piece.shape[0], piece.shape[1], joined.shape[1])
    projected = lax.optimization_barrier(projected).astype(jnp.float32)
    positions_dev, sequences = (projected.shape[0], projected.shape[1])
    head_count = key_width // KEY_DIM
    block_len = math.gcd(positions_dev, 128)
    block_count = positions_dev // block_len

    def blocks(value, channels):
        return value.reshape(block_count, block_len, sequences, head_count, channels)

    query = jax.nn.silu(blocks(projected[..., :key_width], KEY_DIM))
    inkey = floor_gap.reshape(head_count, KEY_DIM) * jax.nn.sigmoid(
        -blocks(projected[..., key_width : 2 * key_width], KEY_DIM)
    )
    log_forget = jnp.log1p(-inkey)
    values = blocks(projected[..., 2 * key_width :], VAL_DIM)
    inside, reach, total_decay, end_state = local_pass(query, inkey, log_forget, values)
    _, incoming = carried_in(
        (total_decay, end_state),
        "sp",
        link_states,
        (jnp.ones_like(total_decay), jnp.zeros_like(end_state)),
    )
    recurrent = inside + read_out(reach, incoming)
    mean_square = jnp.mean(recurrent * recurrent, axis=-1, keepdims=True)
    hidden = recurrent * lax.rsqrt(mean_square + eps_norm) * head_gain.reshape(head_count, VAL_DIM)
    hidden = hidden.astype(jnp.bfloat16).reshape(positions_dev, sequences, head_count * VAL_DIM)
    out_columns = lax.all_gather(w_out, "sp", axis=1, tiled=True)
    piece = hidden
    return lax.psum_scatter(
        jnp.einsum("psh,hd->psd", piece, out_columns, preferred_element_type=jnp.float32).astype(
            jnp.bfloat16
        ),
        "tp",
        scatter_dimension=0,
        tiled=True,
    )


def solution(mesh):
    return jax.shard_map(
        body,
        mesh=mesh,
        in_specs=(
            P(("sp", "tp"), None, None),
            P(),
            P("sp", "tp"),
            P("sp", "tp"),
            P("sp", "tp"),
            P("tp"),
            P("tp"),
            P("tp", "sp"),
        ),
        out_specs=P(("sp", "tp"), None, None),
        check_vma=False,
    )
```

profile of v0, /device:TPU:24, one launch (start us, length us, event | category | flops | bytes accessed | tf_op | source)
XLA Modules:
  0.0 462.1 jit_solution(16212869938098595885)
XLA Ops:
  6.5 1.4 fusion.8
  7.9 2.2 fusion.10
  10.1 0.0 all-gather.15.cloned.1.call-start
  10.2 0.7 all-gather.15.cloned.1.call-update
  10.9 0.0 all-gather.13.cloned.1.call-start
  10.9 0.7 all-gather.13.cloned.1.call-update
  11.6 0.0 all-gather.11.cloned.1.call-start
  11.7 0.5 all-gather.11.cloned.1.call-update
  12.2 0.0 all-gather.19.cloned.1.call-start
  12.3 20.3 %all-gather.9.cloned.1.call-done = bf16[64,4,2048]{2,1,0:T(4,128)(2,1)} async-done(((bf16[32,4,2048]{2,1,0:T(4,128)(2,1)}), bf16[64,4,2048]{2,1,0:T(4,128)(2,1)}) %all-gather.9.cloned.1.call-update) | async-done | bytes 1048592 | tf_op jit(solution)/shard_map/all_gather | solution.py:80
  32.6 1.3 reshape.179
  33.9 49.8 %all-gather.15.cloned.1.call-done = bf16[2048,1024]{1,0:T(8,128)(2,1)} async-done(((bf16[128,1024]{1,0:T(8,128)(2,1)}), bf16[2048,1024]{1,0:T(8,128)(2,1)}) %all-gather.15.cloned.1.call-update) | async-done | bytes 4194320 | tf_op jit(solution)/shard_map/all_gather | solution.py:77
  83.7 3.4 convolution_convert_fusion
  87.1 47.7 %all-gather.13.cloned.1.call-done = bf16[2048,1024]{1,0:T(8,128)(2,1)} async-done(((bf16[128,1024]{1,0:T(8,128)(2,1)}), bf16[2048,1024]{1,0:T(8,128)(2,1)}) %all-gather.13.cloned.1.call-update) | async-done | bytes 4194320 | tf_op jit(solution)/shard_map/all_gather | solution.py:76
  134.8 4.2 convolution_convert_fusion.1
  139.0 46.7 %all-gather.11.cloned.1.call-done = bf16[2048,1024]{1,0:T(8,128)(2,1)} async-done(((bf16[128,1024]{1,0:T(8,128)(2,1)}), bf16[2048,1024]{1,0:T(8,128)(2,1)}) %all-gather.11.cloned.1.call-update) | async-done | bytes 4194320 | tf_op jit(solution)/shard_map/all_gather | solution.py:75
  185.7 3.5 convolution_convert_fusion.2
  189.2 0.1 pad_maximum_fusion
  189.3 0.6 reshape.180
  190.0 0.4 convert_element_type.29
  190.4 0.6 fusion.12
  190.9 1.4 div.47
  192.3 1.4 div.48
  193.7 0.1 slice.17
  193.9 1.1 copy-done.4
  195.0 0.5 fusion.22
  195.5 1.5 reshape.182
  197.0 0.2 reshape.187
  197.2 3.8 fusion.17
  201.0 3.7 convolution_add_fusion
  204.7 0.0 all-gather.17.cloned.1.call-start
  204.8 0.5 all-gather.17.cloned.1.call-update
  205.3 0.2 reduce-scatter.2.cloned.1.call-start
  205.6 4.1 convolution_select_fusion
  209.7 0.7 fusion.30
  210.5 2.5 fusion.6
  212.9 18.4 %all-gather = f32[16,1,4,8,128]{4,3,2,1,0:T(8,128)S(1)} all-gather(f32[1,1,4,8,128]{4,3,2,1,0:T(8,128)S(1)} %get-tuple-element.151), channel_id=2, replica_groups=mesh['sp'=16,'tp'=2] {'sp'}, dimensions={0}, use_global_device_ids=true | all-gather | bytes 278528 | tf_op jit(solution)/shard_map/all_gather | solution.py:18
  231.4 144.0 %all-gather.19.cloned.1.call-done = f32[64,8,128,128]{3,2,1,0:T(8,128)} async-done(((f32[4,8,128,128]{3,2,1,0:T(8,128)}), f32[64,8,128,128]{3,2,1,0:T(8,128)}) %all-gather.19.cloned.1.call-update) | async-done | bytes 33554448 | tf_op jit(solution)/shard_map/all_gather | solution.py:18
  375.4 35.5 %while.9 = (s32[]{:T(128)}, f32[4,8,128,128]{3,2,1,0:T(8,128)S(1)}, s32[]{:T(128)}, f32[16,4,8,128]{3,2,1,0:T(8,128)S(1)}, f32[16,4,8,128,128]{4,3,2,1,0:T(8,128)}, /*index=5*/s32[]{:T(128)}, s32[]{:T(128)}) while((s32[]{:T(128)}, f32[4,8,128,128]{3,2,1,0:T(8,128)S(1)}, s32[]{:T(128)}, f32[16,4,8,128]{3,2,1,0:T(8,128)S(1)}, ...), condition=%wide.region_3.4_spmd.clone, body=%wide.region_2.3_spmd.clone.sunk | while | flops 2097156 | bytes 6340721 | solution.py:30
  375.4 2.2 fusion.44
  377.6 2.2 fusion.44
  379.9 2.2 fusion.44
  382.1 2.2 fusion.44
  384.3 2.2 fusion.44
  386.5 2.2 fusion.44
  388.7 2.2 fusion.44
  391.0 2.2 fusion.44
  393.2 2.2 fusion.44
  395.4 2.2 fusion.44
  397.6 2.2 fusion.44
  399.8 2.2 fusion.44
  402.0 2.2 fusion.44
  404.2 2.2 fusion.44
  406.5 2.2 fusion.44
  408.7 2.2 fusion.44
  410.9 3.8 multiply_reduce_fusion
  414.7 0.3 multiply_convert_fusion
  415.0 0.3 copy.29
  415.4 0.2 reshape.183
  415.6 12.4 %all-gather.17.cloned.1.call-done = bf16[1024,2048]{1,0:T(8,128)(2,1)} async-done(((bf16[1024,128]{1,0:T(8,128)(2,1)}), bf16[1024,2048]{1,0:T(8,128)(2,1)}) %all-gather.17.cloned.1.call-update) | async-done | bytes 4194320 | tf_op jit(solution)/shard_map/all_gather | solution.py:114
  428.0 4.4 fusion.3
  432.4 0.0 reduce-scatter.2.cloned.1.call-update
  432.4 20.6 %reduce-scatter.2.cloned.1.call-done = bf16[32,4,2048]{2,0,1:T(8,128)(2,1)} async-done(((bf16[64,4,2048]{2,0,1:T(8,128)(2,1)}), bf16[32,4,2048]{2,0,1:T(8,128)(2,1)}) %reduce-scatter.2.cloned.1.call-update) | async-done | bytes 524304 | tf_op jit(solution)/shard_map/reduce_scatter | solution.py:116
  453.1 2.2 copy.30
  (42 shorter events, 0.2 us)
Async XLA Ops:
  6.5 26.0 %all-gather.9.cloned.1.call-start = ((), (), s32[]{:S(2)}) async-start(), calls=%async_computation.1 | async-start | bytes 1572864 | tf_op jit(solution)/shard_map/all_gather | solution.py:80
  10.1 73.5 %all-gather.15.cloned.1.call-start = ((), (), s32[]{:S(2)}) async-start(), calls=%async_computation.4 | async-start | bytes 4456448 | tf_op jit(solution)/shard_map/all_gather | solution.py:77
  10.9 123.9 %all-gather.13.cloned.1.call-start = ((), (), s32[]{:S(2)}) async-start(), calls=%async_computation.3 | async-start | bytes 4456448 | tf_op jit(solution)/shard_map/all_gather | solution.py:76
  11.6 174.1 %all-gather.11.cloned.1.call-start = ((), (), s32[]{:S(2)}) async-start(), calls=%async_computation.2 | async-start | bytes 4456448 | tf_op jit(solution)/shard_map/all_gather | solution.py:75
  12.2 363.1 %all-gather.19.cloned.1.call-start = ((), (), s32[]{:S(2)}) async-start(), calls=%async_computation.7 | async-start | bytes 35651584 | tf_op jit(solution)/shard_map/all_gather | solution.py:18
  185.7 3.5 copy-start.5
  190.0 3.9 copy-start
  193.7 1.2 copy-start.4
  193.7 1.2 copy-start.6
  195.0 2.0 slice-start
  197.2 3.8 copy-start.1
  204.7 223.3 %all-gather.17.cloned.1.call-start = ((), (), s32[]{:S(2)}) async-start(), calls=%async_computation.5 | async-start | bytes 4456448 | tf_op jit(solution)/shard_map/all_gather | solution.py:114
  205.3 247.8 %reduce-scatter.2.cloned.1.call-start = ((), (), s32[]{:S(2)}) async-start(), calls=%async_computation.6 | async-start | bytes 1572864 | tf_op jit(solution)/shard_map/reduce_scatter | solution.py:116
  205.6 4.1 copy-start.2
  375.4 35.5 %copy-start.3 = (f32[64,4,8,128]{3,2,1,0:T(8,128)S(1)}, f32[64,4,8,128]{3,2,1,0:T(8,128)}, u32[]{:S(2)}) copy-start(f32[64,4,8,128]{3,2,1,0:T(8,128)} %get-tuple-element.147) | copy-start | bytes 3145732
  410.9 3.8 copy-start.7
Sparse Core Ops, SparseCore 0:
  10.3 22.2 all-gather.8
  34.7 48.9 all-gather.14
  85.8 48.8 all-gather.12
  136.8 48.8 all-gather.10
  204.8 170.4 all-gather.18
  377.4 50.5 all-gather.16
  432.6 20.4 reduce-scatter.1
where the time goes:
time: 465 us; the launch traced here: 462 us
  waiting for transfers between devices  344 us (74%)
  other arithmetic  44 us (9%)
  matrix products  30.4 us (7%)
  blocking collectives  18.4 us (4%)
  between operations  13.7 us (3%)
  local copies, waits for them, and re-layouts  10.6 us (2%)
    all_gather x1, waiting for transfers between devices, carried_in(): everything = jax.tree.map(lambda part: lax.all_gather(part, axis), value)  144 us
    all_gather x1, waiting for transfers between devices, body(): lax.all_gather(w_value, 'sp', axis=0, tiled=True)  49.8 us
    all_gather x1, waiting for transfers between devices, body(): lax.all_gather(w_forget, 'sp', axis=0, tiled=True)  47.7 us
    all_gather x1, waiting for transfers between devices, body(): lax.all_gather(w_query, 'sp', axis=0, tiled=True)  46.7 us
    select_n x16, other arithmetic, hop(): return jax.tree.map(lambda a, b: jnp.where(reached, a, b), new, before)  34.8 us
    reduce_scatter x1, waiting for transfers between devices, body(): lax.psum_scatter(jnp.einsum('psh,hd->psd', piece, out_columns, preferred_...  20.6 us
    all_gather x1, waiting for transfers between devices, body(): piece = lax.all_gather(normed, 'tp', axis=0, tiled=True)  20.3 us
    all_gather x1, blocking collectives, carried_in(): everything = jax.tree.map(lambda part: lax.all_gather(part, axis), value)  18.4 us
  transfers between devices with their start and end apart: 7, of which 7 were waited for; matrix products, arithmetic and copies ran while one was open for 12% of the time, Pallas kernels for 0%

commit v1 on v0

v1 whole, which is shorter than its diff:
```python
import functools
import math

import jax
import jax.numpy as jnp
from jax import lax
from jax.experimental import pallas as pl
from jax.experimental.pallas import tpu as pltpu
from jax.sharding import PartitionSpec as P

KEY_DIM = 128
VAL_DIM = 128
eps_norm = 1e-06
MESH = pl.DeviceIdType.MESH
f32 = jnp.float32
bf16 = jnp.bfloat16


def nt(a, b):
    return lax.dot_general(a, b, (((1,), (1,)), ((), ())), preferred_element_type=f32)


def tn(a, b):
    return lax.dot_general(a, b, (((0,), (0,)), ((), ())), preferred_element_type=f32)


def kernel(
    dims,
    tok, gain, wq, wf, wv, wo, gap, hgain,
    out,
    X, N, W, PJ, IK, CUM, QS, INS, U, DEC, SS, DS, SR, DR, ACC, HB, OB, PB, RSB, RB,
    w_send, w_recv, t_send, t_recv, s_send, s_recv, d_send, d_recv, p_send, p_recv, r_send, r_recv, loc,
):
    n_sp, n_tp, G, C, seqs, ppd, hl, block = dims
    n_o, J, JC = n_sp // G, G * n_tp, G * n_tp // C
    D = tok.shape[1]
    rows = wq.shape[0]
    kw = hl * KEY_DIM
    T = J * ppd
    nb = T // block
    i, t = lax.axis_index("sp"), lax.axis_index("tp")
    o, g = i // G, lax.rem(i, G)
    a, c = g // C, lax.rem(g, C)
    me_j = g * n_tp + t
    me_jj = a * n_tp + t
    partner = o * G + a * C + (1 - c)

    def remote(src, dst, send, recv, sp, tp):
        return pltpu.make_async_remote_copy(
            src_ref=src, dst_ref=dst, send_sem=send, recv_sem=recv, device_id=(sp, tp), device_id_type=MESH
        )

    def away():
        for da in range(G // C):
            for dt in range(n_tp):
                if da or dt:
                    yield da, dt

    def tok_copy(da, dt, sending):
        sign = 1 if sending else -1
        aa = lax.rem(a + sign * da + G // C, G // C)
        tt = lax.rem(t + sign * dt + n_tp, n_tp)
        gg = aa * C + c
        source = me_j if sending else gg * n_tp + tt
        return source, remote(
            tok, X.at[source], t_send.at[da * n_tp + dt], t_recv.at[source], o * G + gg, tt
        )

    for da, dt in away():
        tok_copy(da, dt, True)[1].start()
    own_tok = pltpu.make_async_copy(tok, X.at[me_j], loc.at[4])
    own_tok.start()
    if C > 1:
        to_partner = remote(tok, X.at[me_j], t_send.at[JC], t_recv.at[me_j], partner, t)
        to_partner.start()

    weights = (wf, wv, wq, wo)

    def w_copy(m, source, dest):
        cols = pl.ds(pl.multiple_of(lax.rem(dest, G) * kw, 128), kw)
        return remote(
            weights[m].at[:, cols],
            W.at[m, pl.ds(pl.multiple_of(source * rows, rows), rows), :],
            w_send.at[m, dest], w_recv.at[m, source], dest, t,
        )

    for m in range(4):
        def send_w(k, _, m=m):
            w_copy(m, i, lax.rem(i + k, n_sp)).start()
            return 0
        lax.fori_loop(1, n_sp, send_w, 0)
    own_cols = pl.ds(pl.multiple_of(g * kw, 128), kw)
    own_w = [
        pltpu.make_async_copy(
            weights[m].at[:, own_cols],
            W.at[m, pl.ds(pl.multiple_of(i * rows, rows), rows), :], loc.at[m],
        )
        for m in range(4)
    ]
    for copy in own_w:
        copy.start()

    def wait_w(m):
        def one(k, _):
            src = lax.rem(i + n_sp - k, n_sp)
            back = lax.rem(i, n_sp)
            cols = pl.ds(pl.multiple_of(lax.rem(back, G) * kw, 128), kw)
            remote(
                weights[m].at[:, cols],
                W.at[m, pl.ds(pl.multiple_of(src * rows, rows), rows), :],
                w_send.at[m, src], w_recv.at[m, src], src, t,
            ).wait_recv()
            return 0
        lax.fori_loop(1, n_sp, one, 0)
        own_w[m].wait()

    forwards = []
    for n, (da, dt) in enumerate(away()):
        source, copy = tok_copy(da, dt, False)
        copy.wait_recv()
        if C > 1:
            fwd = remote(X.at[source], X.at[source], t_send.at[JC + 1 + n], t_recv.at[source], partner, t)
            fwd.start()
            forwards.append(fwd)
    own_tok.wait()
    if C > 1:
        for da in range(G // C):
            for dt in range(n_tp):
                aa = lax.rem(a + da, G // C)
                tt = lax.rem(t + dt, n_tp)
                source = (aa * C + 1 - c) * n_tp + tt
                remote(tok, X.at[source], t_send.at[JC], t_recv.at[source], partner, t).wait_recv()

    step = math.gcd(seqs * ppd, 16)
    gain_row = gain[...]

    def norm_block(j, _):
        def norm_rows(r, _):
            where = pl.ds(pl.multiple_of(r * step, step), step)
            x = X[j, where, :].astype(f32)
            scale = lax.rsqrt(jnp.mean(x * x, axis=-1, keepdims=True) + eps_norm)
            N[j, where, :] = (x * scale * gain_row).astype(bf16)
            return 0
        lax.fori_loop(0, seqs * ppd // step, norm_rows, 0)
        return 0
    lax.fori_loop(0, J, norm_block, 0)

    per = max(1, min(J, 512 // (seqs * ppd)))

    def project(m):
        def tile(r, _):
            where = pl.ds(r * per, per)
            x = N[where].reshape(per * seqs * ppd, D)
            y = jnp.dot(x, W[m], preferred_element_type=f32).astype(bf16).astype(f32)
            PJ[m, where] = y.reshape(per, seqs, ppd, kw)
            return 0
        lax.fori_loop(0, J // per, tile, 0)

    wait_w(0)
    project(0)
    wait_w(1)
    project(1)

    gap_row = gap[:, own_cols]
    row_id = lax.broadcasted_iota(jnp.int32, (block, block), 0)
    col_id = lax.broadcasted_iota(jnp.int32, (block, block), 1)
    causal = row_id >= col_id
    ones = jnp.where(causal, 1.0, 0.0).astype(bf16)

    def head(h):
        return slice(h * KEY_DIM, (h + 1) * KEY_DIM)

    def state_copies(s, k, dest_o, src_o):
        sp = dest_o * G + g
        return (
            remote(SS.at[s], SR.at[src_o, s], s_send.at[k, s], s_recv.at[src_o, s], sp, t),
            remote(DS.at[s], DR.at[src_o, s], d_send.at[k, s], d_recv.at[src_o, s], sp, t),
        )

    def key_side(s, _):
        f = PJ[0, :, s].reshape(T, kw)
        v = PJ[1, :, s].reshape(T, kw).astype(bf16)
        inkey = gap_row * jax.nn.sigmoid(-f)
        log_forget = jnp.log1p(-inkey)
        IK[s] = inkey
        ends = [None] * hl
        total = None
        for b in range(nb):
            rs = slice(b * block, (b + 1) * block)
            lf = log_forget[rs]
            high = lf.astype(bf16)
            low = (lf - high.astype(f32)).astype(bf16)
            cum = jnp.dot(ones, high, preferred_element_type=f32) + jnp.dot(
                ones, low, preferred_element_type=f32
            )
            CUM[s, rs, :] = cum
            final = cum[block - 1 : block, :]
            dec = jnp.exp(final)
            DEC[s, b] = jnp.broadcast_to(dec, (8, kw))
            kf = (inkey[rs] * jnp.exp(final - cum)).astype(bf16)
            vb = v[rs]
            total = dec if total is None else total * dec
            for h in range(hl):
                u = tn(vb[:, head(h)], kf[:, head(h)])
                U[s, b, h] = u
                ends[h] = u if ends[h] is None else ends[h] * dec[:, head(h)] + u
        for h in range(hl):
            SS[s, h] = ends[h].astype(bf16)
        DS[s] = jnp.broadcast_to(total, (8, kw))

        def send(k, _):
            @pl.when(o + k < n_o)
            def _():
                for copy in state_copies(s, k, o + k, o):
                    copy.start()
            return 0
        lax.fori_loop(1, n_o, send, 0)
        return 0
    lax.fori_loop(0, seqs, key_side, 0)

    wait_w(2)
    project(2)

    def query_side(s, _):
        q = PJ[2, :, s].reshape(T, kw)
        v = PJ[1, :, s].reshape(T, kw).astype(bf16)
        q = q * jax.nn.sigmoid(q)
        for b in range(nb):
            rs = slice(b * block, (b + 1) * block)
            cum = CUM[s, rs, :]
            qs = (q[rs] * jnp.exp(cum)).astype(bf16)
            ks = (IK[s, rs, :] * jnp.exp(-cum)).astype(bf16)
            QS[s, rs, :] = qs
            vb = v[rs]
            for h in range(hl):
                scores = jnp.where(causal, nt(qs[:, head(h)], ks[:, head(h)]), 0.0).astype(bf16)
                INS[s, rs, head(h)] = jnp.dot(scores, vb[:, head(h)], preferred_element_type=f32)
        return 0
    lax.fori_loop(0, seqs, query_side, 0)

    wait_w(3)
    hg_row = hgain[:, own_cols]
    wide = math.gcd(D, 512)

    def pair_copy(s):
        return remote(OB.at[1 - c, :, s], PB.at[:, s], p_send.at[s], p_recv.at[s], partner, t)

    def plane_copy(da, dt, s, sending):
        sign = 1 if sending else -1
        aa = lax.rem(a + sign * da + G // C, G // C)
        tt = lax.rem(t + sign * dt + n_tp, n_tp)
        other = aa * n_tp + tt
        src, slot = (other, me_jj) if sending else (me_jj, other)
        return remote(
            RSB.at[src, s], RB.at[slot, s], r_send.at[da * n_tp + dt, s], r_recv.at[slot, s],
            o * G + aa * C + c, tt,
        )

    def finish(s):
        for h in range(hl):
            ACC[h] = jnp.zeros((VAL_DIM, KEY_DIM), f32)

        def earlier(k, _):
            @pl.when(k < o)
            def _():
                for copy in state_copies(s, 0, o, k):
                    copy.wait_recv()
                dec = DR[k, s][0:1, :]
                for h in range(hl):
                    ACC[h] = ACC[h] * dec[:, head(h)] + SR[k, s, h].astype(f32)
            return 0
        lax.fori_loop(0, n_o - 1, earlier, 0)
        for h in range(hl):
            state = ACC[h]
            for b in range(nb):
                rs = slice(b * block, (b + 1) * block)
                r = INS[s, rs, head(h)] + nt(QS[s, rs, head(h)], state.astype(bf16))
                scale = lax.rsqrt(jnp.mean(r * r, axis=-1, keepdims=True) + eps_norm)
                HB[rs, head(h)] = (r * scale * hg_row[:, head(h)]).astype(bf16)
                if b + 1 < nb:
                    state = state * DEC[s, b][0:1, head(h)] + U[s, b, h]
        hidden = HB[...]

        def columns(n, _):
            cs = pl.ds(pl.multiple_of(n * wide, wide), wide)
            y = nt(hidden, W[3, cs, :]).reshape(G // C, C, n_tp, ppd, wide)
            for par in range(C):
                OB[par, :, s, :, cs] = y[:, par].reshape(JC, ppd, wide).astype(bf16)
            return 0
        lax.fori_loop(0, D // wide, columns, 0)
        if C > 1:
            pair_copy(s).start()

    def reduce(s):
        if C > 1:
            pair_copy(s).wait_recv()

        def one(jj, _):
            if C > 1:
                RSB[jj, s] = (OB[c, jj, s].astype(f32) + PB[jj, s].astype(f32)).astype(bf16)
            else:
                RSB[jj, s] = OB[0, jj, s]
            return 0
        lax.fori_loop(0, JC, one, 0)
        for da, dt in away():
            plane_copy(da, dt, s, True).start()
        RB[me_jj, s] = RSB[me_jj, s]

    def pipeline(s, _):
        @pl.when(s < seqs)
        def _():
            finish(s)

        @pl.when(s > 0)
        def _():
            reduce(s - 1)
        return 0
    lax.fori_loop(0, seqs + 1, pipeline, 0)

    def last(s, _):
        for da, dt in away():
            plane_copy(da, dt, s, False).wait_recv()
        total = RB[0, s].astype(f32)
        for jj in range(1, JC):
            total = total + RB[jj, s].astype(f32)
        out[s] = total.astype(bf16)
        return 0
    lax.fori_loop(0, seqs, last, 0)

    for da, dt in away():
        tok_copy(da, dt, True)[1].wait_send()
    if C > 1:
        to_partner.wait_send()
        for fwd in forwards:
            fwd.wait_send()
    for m in range(4):
        def sent_w(k, _, m=m):
            w_copy(m, i, lax.rem(i + k, n_sp)).wait_send()
            return 0
        lax.fori_loop(1, n_sp, sent_w, 0)

    def sent(s, _):
        def states(k, _):
            @pl.when(o + k < n_o)
            def _():
                for copy in state_copies(s, k, o + k, o):
                    copy.wait_send()
            return 0
        lax.fori_loop(1, n_o, states, 0)
        if C > 1:
            pair_copy(s).wait_send()
        for da, dt in away():
            plane_copy(da, dt, s, True).wait_send()
        return 0
    lax.fori_loop(0, seqs, sent, 0)


def body(n_sp, n_tp, tokens, norm_gain, w_query, w_forget, w_value, floor_gap, head_gain, w_out):
    ppd, seqs, D = tokens.shape
    rows, width = w_query.shape
    heads = width // KEY_DIM
    G = math.gcd(math.gcd(n_sp, 4), max(1, heads // 2))
    C = 2 if G % 2 == 0 else 1
    hl = heads // G
    kw = hl * KEY_DIM
    n_o, J = n_sp // G, G * n_tp
    JC = J // C
    T = J * ppd
    block = math.gcd(T, 128)
    nb = T // block
    dims = (n_sp, n_tp, G, C, seqs, ppd, hl, block)
    vmem = pl.BlockSpec(memory_space=pltpu.VMEM)
    dma = pltpu.SemaphoreType.DMA
    result = pl.pallas_call(
        functools.partial(kernel, dims),
        out_shape=jax.ShapeDtypeStruct((seqs, ppd, D), bf16),
        in_specs=[vmem] * 8,
        out_specs=vmem,
        scratch_shapes=[
            pltpu.VMEM((J, seqs * ppd, D), bf16),
            pltpu.VMEM((J, seqs * ppd, D), bf16),
            pltpu.VMEM((4, n_sp * rows, kw), bf16),
            pltpu.VMEM((3, J, seqs, ppd, kw), f32),
            pltpu.VMEM((seqs, T, kw), f32),
            pltpu.VMEM((seqs, T, kw), f32),
            pltpu.VMEM((seqs, T, kw), bf16),
            pltpu.VMEM((seqs, T, kw), f32),
            pltpu.VMEM((seqs, nb, hl, VAL_DIM, KEY_DIM), f32),
            pltpu.VMEM((seqs, nb, 8, kw), f32),
            pltpu.VMEM((seqs, hl, VAL_DIM, KEY_DIM), bf16),
            pltpu.VMEM((seqs, 8, kw), f32),
            pltpu.VMEM((n_o, seqs, hl, VAL_DIM, KEY_DIM), bf16),
            pltpu.VMEM((n_o, seqs, 8, kw), f32),
            pltpu.VMEM((hl, VAL_DIM, KEY_DIM), f32),
            pltpu.VMEM((T, kw), bf16),
            pltpu.VMEM((C, JC, seqs, ppd, D), bf16),
            pltpu.VMEM((JC, seqs, ppd, D), bf16),
            pltpu.VMEM((JC, seqs, ppd, D), bf16),
            pltpu.VMEM((JC, seqs, ppd, D), bf16),
            dma((4, n_sp)), dma((4, n_sp)),
            dma((2 * JC + 1,)), dma((J,)),
            dma((n_o, seqs)), dma((n_o, seqs)),
            dma((n_o, seqs)), dma((n_o, seqs)),
            dma((seqs,)), dma((seqs,)),
            dma((JC, seqs)), dma((JC, seqs)),
            dma((5,)),
        ],
        compiler_params=pltpu.CompilerParams(has_side_effects=True, vmem_limit_bytes=62 * 1024 * 1024),
        name="block",
    )(
        tokens.transpose(1, 0, 2).reshape(seqs * ppd, D),
        norm_gain.reshape(1, D), w_query, w_forget, w_value, w_out.T,
        floor_gap.reshape(1, width), head_gain.reshape(1, width),
    )
    return result.transpose(1, 0, 2)


def solution(mesh):
    return jax.shard_map(
        functools.partial(body, mesh.shape["sp"], mesh.shape["tp"]),
        mesh=mesh,
        in_specs=(
            P(("sp", "tp"), None, None),
            P(),
            P("sp", "tp"),
            P("sp", "tp"),
            P("sp", "tp"),
            P("tp"),
            P("tp"),
            P("tp", "sp"),
        ),
        out_specs=P(("sp", "tp"), None, None),
        check_vma=False,
    )
```

time: 465 us -> 157 us (0.34)
  waiting for transfers between devices: 344 us -> 0 us
  Pallas kernels: 0 us -> 151 us
  other arithmetic: 44 us -> 0 us
  matrix products: 30.4 us -> 0 us
  blocking collectives: 18.4 us -> 0 us
  between operations: 13.7 us -> 0.01 us
  local copies, waits for them, and re-layouts: 10.6 us -> 5.17 us
    all_gather x6 -> x0, waiting for transfers between devices: 321 us -> none  [the longest x1 144 us: carried_in(): everything = jax.tree.map(lambda part: lax.all_gather(part, axis), value)]
    pallas_call x0 -> x1, Pallas kernels: none -> 151 us  [body(): pl.pallas_call(functools.partial(kernel, dims), out_shape=jax.ShapeDtypeS...]
    select_n x16 -> x0, other arithmetic: 34.8 us -> none  [hop(): return jax.tree.map(lambda a, b: jnp.where(reached, a, b), new, before)]
    dot_general x9 -> x0, matrix products: 30.4 us -> none  [the longest x3 11.2 us: body(): jnp.dot(flat_rows, weight, preferred_element_type=jnp.float32)]
    reduce_scatter x1 -> x0, waiting for transfers between devices: 20.6 us -> none  [body(): lax.psum_scatter(jnp.einsum('psh,hd->psd', piece, out_columns, preferred_...]
    all_gather x1 -> x0, blocking collectives: 18.4 us -> none  [carried_in(): everything = jax.tree.map(lambda part: lax.all_gather(part, axis), value)]
  transfers between devices with their start and end apart: 7 -> 0, of which waited for: 7 -> 0; matrix products, arithmetic and copies ran while one was open for 12% -> 0% of each run, Pallas kernels for 0% -> 0%
where the time goes in v1:
time: 157 us; the launch traced here: 156 us
  Pallas kernels  151 us (96%)
  local copies, waits for them, and re-layouts  5.17 us (3%)
    pallas_call x1, Pallas kernels, body(): pl.pallas_call(functools.partial(kernel, dims), out_shape=jax.ShapeDtypeS...  151 us

profile of v1, /device:TPU:24, one launch (start us, length us, event | category | flops | bytes accessed | tf_op | source)
XLA Modules:
  0.0 156.4 jit_solution(12173692408044470458)
XLA Ops:
  0.0 0.0 copy-start
  0.0 1.8 %copy.10 = bf16[1024,128]{0,1:T(8,128)(2,1)} copy(bf16[1024,128]{1,0:T(8,128)(2,1)} %param.15) | data formatting | bytes 524288 | tf_op args[7]
  1.8 0.0 copy-done
  1.8 1.1 copy.9
  2.9 151.2 %block.1 = bf16[4,32,2048]{2,1,0:T(8,128)(2,1)} custom-call(bf16[128,2048]{1,0:T(8,128)(2,1)} %bitcast.8, f32[1,2048]{1,0:T(1,128)} %bitcast.11, bf16[128,1024]{1,0:T(8,128)(2,1)} %wq.1, bf16[128,1024]{1,0:T(8,128)(2,1)} %wf.1, bf16[128,1024]{1,0:T(8,128)(2,1)} %wv.1, bf16[128,1024]{1,0:T(8,128)(2,1)} %bitcast.9, f32[1,1024]{1,0:T(1,128)} %bitcast.12, ...), custom_call_target="tpu_custom_call" | custom-call | tf_op jit(solution)/shard_map/block/pallas_call | solution.py:374
  154.2 2.2 %copy.11 = bf16[32,4,2048]{2,1,0:T(4,128)(2,1)} copy(bf16[32,4,2048]{2,0,1:T(8,128)(2,1)} %bitcast.7) | data formatting | bytes 1048576 | tf_op jit(solution)/shard_map/transpose | solution.py:415
Async XLA Ops:
  0.0 1.8 %copy-start = (bf16[32,4,2048]{2,1,0:T(4,128)(2,1)S(1)}, bf16[32,4,2048]{2,1,0:T(4,128)(2,1)}, u32[]{:S(2)}) copy-start(bf16[32,4,2048]{2,1,0:T(4,128)(2,1)} %param.8) | copy-start | bytes 1572868

commit v2 on v1

--- a/solution.py
+++ b/solution.py
@@ -28,8 +28,8 @@
     dims,
     tok, gain, wq, wf, wv, wo, gap, hgain,
     out,
-    X, N, W, PJ, IK, CUM, QS, INS, U, DEC, SS, DS, SR, DR, ACC, HB, OB, PB, RSB, RB,
-    w_send, w_recv, t_send, t_recv, s_send, s_recv, d_send, d_recv, p_send, p_recv, r_send, r_recv, loc,
+    X, N, W, PJ, IK, CUM, QS, INS, U, DEC, EL, DT, SS, SR, ACC, HB, OB, PB, RSB, RB,
+    w_send, w_recv, z_send, z_recv, t_send, t_recv, s_send, s_recv, p_send, p_recv, r_send, r_recv, loc,
 ):
     n_sp, n_tp, G, C, seqs, ppd, hl, block = dims
     n_o, J, JC = n_sp // G, G * n_tp, G * n_tp // C
@@ -66,53 +66,92 @@
             tok, X.at[source], t_send.at[da * n_tp + dt], t_recv.at[source], o * G + gg, tt
         )
 
+    weights = (wf, wv, wq, wo)
+    n_w = len(weights)
+
+    def block_of(m, b):
+        return W.at[m, pl.ds(pl.multiple_of(b * G * rows, G * rows), G * rows), :]
+
+    def slice_of(m, source):
+        return W.at[m, pl.ds(pl.multiple_of(source * rows, rows), rows), :]
+
+    def plane_w(m, k):
+        gg = lax.rem(g + k, G)
+        cols = pl.ds(pl.multiple_of(gg * kw, 128), kw)
+        return remote(
+            weights[m].at[:, cols], slice_of(m, i), w_send.at[m, k], w_recv.at[m, k], o * G + gg, t
+        )
+
+    def line_w(m, b, way):
+        return remote(
+            block_of(m, b), block_of(m, b), z_send.at[way, m, b], z_recv.at[m, b],
+            (o + 1 - 2 * way) * G + g, t,
+        )
+
+    own_cols = pl.ds(pl.multiple_of(g * kw, 128), kw)
+    for m in range(n_w):
+        for k in range(1, G):
+            plane_w(m, k).start()
+        pltpu.make_async_copy(weights[m].at[:, own_cols], slice_of(m, i), loc.at[m]).start()
+
     for da, dt in away():
         tok_copy(da, dt, True)[1].start()
-    own_tok = pltpu.make_async_copy(tok, X.at[me_j], loc.at[4])
+    own_tok = pltpu.make_async_copy(tok, X.at[me_j], loc.at[n_w])
     own_tok.start()
     if C > 1:
         to_partner = remote(tok, X.at[me_j], t_send.at[JC], t_recv.at[me_j], partner, t)
         to_partner.start()
 
-    weights = (wf, wv, wq, wo)
-
-    def w_copy(m, source, dest):
-        cols = pl.ds(pl.multiple_of(lax.rem(dest, G) * kw, 128), kw)
-        return remote(
-            weights[m].at[:, cols],
-            W.at[m, pl.ds(pl.multiple_of(source * rows, rows), rows), :],
-            w_send.at[m, dest], w_recv.at[m, source], dest, t,
-        )
-
-    for m in range(4):
-        def send_w(k, _, m=m):
-            w_copy(m, i, lax.rem(i + k, n_sp)).start()
-            return 0
-        lax.fori_loop(1, n_sp, send_w, 0)
-    own_cols = pl.ds(pl.multiple_of(g * kw, 128), kw)
-    own_w = [
-        pltpu.make_async_copy(
-            weights[m].at[:, own_cols],
-            W.at[m, pl.ds(pl.multiple_of(i * rows, rows), rows), :], loc.at[m],
-        )
-        for m in range(4)
-    ]
-    for copy in own_w:
-        copy.start()
-
-    def wait_w(m):
-        def one(k, _):
-            src = lax.rem(i + n_sp - k, n_sp)
-            back = lax.rem(i, n_sp)
-            cols = pl.ds(pl.multiple_of(lax.rem(back, G) * kw, 128), kw)
-            remote(
-                weights[m].at[:, cols],
-                W.at[m, pl.ds(pl.multiple_of(src * rows, rows), rows), :],
-                w_send.at[m, src], w_recv.at[m, src], src, t,
-            ).wait_recv()
-            return 0
-        lax.fori_loop(1, n_sp, one, 0)
-        own_w[m].wait()
+    def stage(d):
+        def first(m):
+            for k in range(1, G):
+                gg = lax.rem(g - k + G, G)
+                here = slice_of(m, o * G + gg)
+                remote(here, here, w_send.at[m, k], w_recv.at[m, k], o * G + gg, t).wait_recv()
+            pltpu.make_async_copy(slice_of(m, i), slice_of(m, i), loc.at[m]).wait()
+
+            @pl.when(o + 1 < n_o)
+            def _():
+                line_w(m, o, 0).start()
+
+            @pl.when(o > 0)
+            def _():
+                line_w(m, o, 1).start()
+
+        def hop(r, _):
+            m = d - r
+
+            @pl.when((m >= 0) & (m < n_w) & (o - r >= 0))
+            def _():
+                line_w(m, o - r, 1).wait_recv()
+
+                @pl.when(o + 1 < n_o)
+                def _():
+                    line_w(m, o - r, 0).start()
+
+            @pl.when((m >= 0) & (m < n_w) & (o + r < n_o))
+            def _():
+                line_w(m, o + r, 0).wait_recv()
+
+                @pl.when(o > 0)
+                def _():
+                    line_w(m, o + r, 1).start()
+            return 0
+
+        if isinstance(d, int):
+            if d < n_w:
+                first(d)
+        else:
+            @pl.when(d < n_w)
+            def _():
+                first(d)
+        lax.fori_loop(1, n_o, hop, 0)
+
+    def early(d, _):
+        stage(d)
+        return 0
+    lax.fori_loop(0, n_o - 1, early, 0)
+    stage(n_o - 1)
 
     forwards = []
     for n, (da, dt) in enumerate(away()):
@@ -156,9 +195,8 @@
             return 0
         lax.fori_loop(0, J // per, tile, 0)
 
-    wait_w(0)
     project(0)
-    wait_w(1)
+    stage(n_o)
     project(1)
 
     gap_row = gap[:, own_cols]
@@ -170,12 +208,20 @@
     def head(h):
         return slice(h * KEY_DIM, (h + 1) * KEY_DIM)
 
-    def state_copies(s, k, dest_o, src_o):
-        sp = dest_o * G + g
-        return (
-            remote(SS.at[s], SR.at[src_o, s], s_send.at[k, s], s_recv.at[src_o, s], sp, t),
-            remote(DS.at[s], DR.at[src_o, s], d_send.at[k, s], d_recv.at[src_o, s], sp, t),
-        )
+    def chain_copy(s):
+        return remote(SS.at[s], SR.at[s], s_send.at[s], s_recv.at[s], (o + 1) * G + g, t)
+
+    def chain(s):
+        @pl.when(o > 0)
+        def _():
+            chain_copy(s).wait_recv()
+
+            @pl.when(o + 1 < n_o)
+            def _():
+                for h in range(hl):
+                    incoming = SR[s, h].astype(f32)
+                    SS[s, h] = (incoming * DT[s][0:1, head(h)] + EL[s, h]).astype(bf16)
+                chain_copy(s).start()
 
     def key_side(s, _):
         f = PJ[0, :, s].reshape(T, kw)
@@ -205,20 +251,18 @@
                 U[s, b, h] = u
                 ends[h] = u if ends[h] is None else ends[h] * dec[:, head(h)] + u
         for h in range(hl):
-            SS[s, h] = ends[h].astype(bf16)
-        DS[s] = jnp.broadcast_to(total, (8, kw))
-
-        def send(k, _):
-            @pl.when(o + k < n_o)
-            def _():
-                for copy in state_copies(s, k, o + k, o):
-                    copy.start()
-            return 0
-        lax.fori_loop(1, n_o, send, 0)
+            EL[s, h] = ends[h]
+        DT[s] = jnp.broadcast_to(total, (8, kw))
+
+        @pl.when((o == 0) & (n_o > 1))
+        def _():
+            for h in range(hl):
+                SS[s, h] = ends[h].astype(bf16)
+            chain_copy(s).start()
         return 0
     lax.fori_loop(0, seqs, key_side, 0)
 
-    wait_w(2)
+    stage(n_o + 1)
     project(2)
 
     def query_side(s, _):
@@ -235,10 +279,11 @@
             for h in range(hl):
                 scores = jnp.where(causal, nt(qs[:, head(h)], ks[:, head(h)]), 0.0).astype(bf16)
                 INS[s, rs, head(h)] = jnp.dot(scores, vb[:, head(h)], preferred_element_type=f32)
+        chain(s)
         return 0
     lax.fori_loop(0, seqs, query_side, 0)
 
-    wait_w(3)
+    stage(n_o + 2)
     hg_row = hgain[:, own_cols]
     wide = math.gcd(D, 512)
 
@@ -257,19 +302,12 @@
         )
 
     def finish(s):
-        for h in range(hl):
-            ACC[h] = jnp.zeros((VAL_DIM, KEY_DIM), f32)
-
-        def earlier(k, _):
-            @pl.when(k < o)
-            def _():
-                for copy in state_copies(s, 0, o, k):
-                    copy.wait_recv()
-                dec = DR[k, s][0:1, :]
-                for h in range(hl):
-                    ACC[h] = ACC[h] * dec[:, head(h)] + SR[k, s, h].astype(f32)
-            return 0
-        lax.fori_loop(0, n_o - 1, earlier, 0)
+        ACC[...] = jnp.zeros_like(ACC)
+
+        @pl.when(o > 0)
+        def _():
+            ACC[...] = SR[s].astype(f32)
+
         for h in range(hl):
             state = ACC[h]
             for b in range(nb):
@@ -333,20 +371,25 @@
         to_partner.wait_send()
         for fwd in forwards:
             fwd.wait_send()
-    for m in range(4):
-        def sent_w(k, _, m=m):
-            w_copy(m, i, lax.rem(i + k, n_sp)).wait_send()
-            return 0
-        lax.fori_loop(1, n_sp, sent_w, 0)
+    for m in range(n_w):
+        for k in range(1, G):
+            plane_w(m, k).wait_send()
+
+        def sent_w(b, _, m=m):
+            @pl.when((b <= o) & (o + 1 < n_o))
+            def _():
+                line_w(m, b, 0).wait_send()
+
+            @pl.when((b >= o) & (o > 0))
+            def _():
+                line_w(m, b, 1).wait_send()
+            return 0
+        lax.fori_loop(0, n_o, sent_w, 0)
 
     def sent(s, _):
-        def states(k, _):
-            @pl.when(o + k < n_o)
-            def _():
-                for copy in state_copies(s, k, o + k, o):
-                    copy.wait_send()
-            return 0
-        lax.fori_loop(1, n_o, states, 0)
+        @pl.when(o + 1 < n_o)
+        def _():
+            chain_copy(s).wait_send()
         if C > 1:
             pair_copy(s).wait_send()
         for da, dt in away():
@@ -387,20 +430,20 @@
             pltpu.VMEM((seqs, T, kw), f32),
             pltpu.VMEM((seqs, nb, hl, VAL_DIM, KEY_DIM), f32),
             pltpu.VMEM((seqs, nb, 8, kw), f32),
+            pltpu.VMEM((seqs, hl, VAL_DIM, KEY_DIM), f32),
+            pltpu.VMEM((seqs, 8, kw), f32),
             pltpu.VMEM((seqs, hl, VAL_DIM, KEY_DIM), bf16),
-            pltpu.VMEM((seqs, 8, kw), f32),
-            pltpu.VMEM((n_o, seqs, hl, VAL_DIM, KEY_DIM), bf16),
-            pltpu.VMEM((n_o, seqs, 8, kw), f32),
+            pltpu.VMEM((seqs, hl, VAL_DIM, KEY_DIM), bf16),
             pltpu.VMEM((hl, VAL_DIM, KEY_DIM), f32),
             pltpu.VMEM((T, kw), bf16),
             pltpu.VMEM((C, JC, seqs, ppd, D), bf16),
             pltpu.VMEM((JC, seqs, ppd, D), bf16),
             pltpu.VMEM((JC, seqs, ppd, D), bf16),
             pltpu.VMEM((JC, seqs, ppd, D), bf16),
-            dma((4, n_sp)), dma((4, n_sp)),
+            dma((4, G)), dma((4, G)),
+            dma((2, 4, n_o)), dma((4, n_o)),
             dma((2 * JC + 1,)), dma((J,)),
-            dma((n_o, seqs)), dma((n_o, seqs)),
-            dma((n_o, seqs)), dma((n_o, seqs)),
+            dma((seqs,)), dma((seqs,)),
             dma((seqs,)), dma((seqs,)),
             dma((JC, seqs)), dma((JC, seqs)),
             dma((5,)),

time: 157 us -> 122 us (0.78)
  Pallas kernels: 151 us -> 117 us
    pallas_call x1, Pallas kernels: 151 us -> 117 us  [body(): pl.pallas_call(functools.partial(kernel, dims), out_shape=jax.ShapeDtypeS...]
where the time goes in v2:
time: 122 us
  Pallas kernels  117 us (96%)
  local copies, waits for them, and re-layouts  5.17 us (4%)
    pallas_call x1, Pallas kernels, body(): pl.pallas_call(functools.partial(kernel, dims), out_shape=jax.ShapeDtypeS...  117 us

profile of v2, /device:TPU:24, one launch (start us, length us, event | category | flops | bytes accessed | tf_op | source)
XLA Modules:
  0.0 122.2 jit_solution(10674865114745918377)
XLA Ops:
  0.0 0.0 copy-start
  0.0 1.8 %copy.10 = bf16[1024,128]{0,1:T(8,128)(2,1)} copy(bf16[1024,128]{1,0:T(8,128)(2,1)} %param.15) | data formatting | bytes 524288 | tf_op args[7]
  1.8 0.0 copy-done
  1.8 1.1 copy.9
  2.9 117.0 %block.1 = bf16[4,32,2048]{2,1,0:T(8,128)(2,1)} custom-call(bf16[128,2048]{1,0:T(8,128)(2,1)} %bitcast.8, f32[1,2048]{1,0:T(1,128)} %bitcast.11, bf16[128,1024]{1,0:T(8,128)(2,1)} %wq.1, bf16[128,1024]{1,0:T(8,128)(2,1)} %wf.1, bf16[128,1024]{1,0:T(8,128)(2,1)} %wv.1, bf16[128,1024]{1,0:T(8,128)(2,1)} %bitcast.9, f32[1,1024]{1,0:T(1,128)} %bitcast.12, ...), custom_call_target="tpu_custom_call" | custom-call | tf_op jit(solution)/shard_map/block/pallas_call | solution.py:417
  120.0 2.2 %copy.11 = bf16[32,4,2048]{2,1,0:T(4,128)(2,1)} copy(bf16[32,4,2048]{2,0,1:T(8,128)(2,1)} %bitcast.7) | data formatting | bytes 1048576 | tf_op jit(solution)/shard_map/transpose | solution.py:458
Async XLA Ops:
  0.0 1.8 %copy-start = (bf16[32,4,2048]{2,1,0:T(4,128)(2,1)S(1)}, bf16[32,4,2048]{2,1,0:T(4,128)(2,1)}, u32[]{:S(2)}) copy-start(bf16[32,4,2048]{2,1,0:T(4,128)(2,1)} %param.8) | copy-start | bytes 1572868
